TPU v7x, 32 devices: a whole 2x2x4 slice. The times are simulated.
32 devices in a mesh: sp: 16 (over z, y, x), tp: 2 (over core).
Axes of the slice: x: 2, y: 2, z: 4, core: 2. Of those that a mesh axis runs over, the one named last changes fastest.
Arguments:
- tokens: bfloat16 [16384, 2048], P('sp', 'tp'), may hold values from -6 to 6
- norm_gain: float32 [2048], replicated, may hold values from 0.1 to 1.9
- w_query: bfloat16 [2048, 1024], P('sp', 'tp'), may hold values from -0.125 to 0.125
- w_key: bfloat16 [2048, 512], P('sp', 'tp'), may hold values from -0.125 to 0.125
- w_value: bfloat16 [2048, 512], P('sp', 'tp'), may hold values from -0.125 to 0.125
- w_glu_a: bfloat16 [2048, 1024], P('sp', 'tp'), may hold values from -0.125 to 0.125
- w_glu_b: bfloat16 [2048, 1024], P('sp', 'tp'), may hold values from -0.125 to 0.125
- q_gain: float32 [64], replicated, may hold values from 0.8 to 7
- k_gain: float32 [64], replicated, may hold values from 0.8 to 7
- sink_logit: float32 [16], P('tp'), may hold values from 1 to 4
- conv_taps: float32 [31, 1024], P(None, 'tp'), may hold values from -1 to 1
- chan_gain: float32 [1024], P('tp'), may hold values from 0.1 to 1.9
- chan_bias: float32 [1024], P('tp'), may hold values from -3 to 3
- w_attn_back: bfloat16 [2048, 1024], P('sp', 'tp'), may hold values from -0.1875 to 0.1875
- w_conv_back: bfloat16 [2048, 1024], P('sp', 'tp'), may hold values from -0.1875 to 0.1875
Outputs:
- mixed: bfloat16 [16384, 2048], P(('sp', 'tp'))
- log_weight: float32 [16, 16384], P('tp', 'sp')
All inputs are finite; a program needn't handle non-finite values.
Results may differ from a plain program's by a relative error of at most 0.014.
The roundings to bfloat16 on the way count: a program that leaves them out, or rounds other values in their place, can miss the bound.
Values may be sent and summed in bfloat16 or wider, within the bound.
A program may use at most 128 MiB of HBM per device.

v0:
```python
import jax
import jax.numpy as jnp
from jax import lax
from jax.sharding import PartitionSpec as P

HEAD = 64
CH = 1024
KW = 31
WINDOW = 128
EPS = 1e-06


def passed_along(value, axis, steps):
    count = lax.axis_size(axis)
    leading, last = (max(0, -steps), min(count, count - steps))
    return lax.ppermute(value, axis, [(source, source + steps) for source in range(leading, last)])


def row_norm(inputs, scale_vec):
    squares = jnp.mean(inputs * inputs, axis=-1, keepdims=True)
    return inputs * lax.rsqrt(squares + EPS) * scale_vec


def local(
    tokens,
    norm_gain,
    w_query,
    w_key,
    w_value,
    w_glu_a,
    w_glu_b,
    q_gain,
    k_gain,
    sink_logit,
    conv_taps,
    chan_gain,
    chan_bias,
    w_attn_back,
    w_conv_back,
):
    row_count = tokens.shape[0]
    q_local = w_query.shape[1] // HEAD
    kv_local = w_key.shape[1] // HEAD
    group_size = q_local // kv_local
    kv_width = kv_local * HEAD
    gathered = lax.all_gather(tokens, "tp", axis=1, tiled=True)
    normed = row_norm(gathered.astype(jnp.float32), norm_gain).astype(jnp.bfloat16)
    whole_rows = (
        lax.all_gather(w_query, "sp", axis=0, tiled=True),
        lax.all_gather(w_key, "sp", axis=0, tiled=True),
        lax.all_gather(w_value, "sp", axis=0, tiled=True),
        lax.all_gather(w_glu_a, "sp", axis=0, tiled=True),
        lax.all_gather(w_glu_b, "sp", axis=0, tiled=True),
        lax.all_gather(w_attn_back, "sp", axis=0, tiled=True),
        lax.all_gather(w_conv_back, "sp", axis=0, tiled=True),
    )
    projected = tuple(
        (jnp.dot(normed, weight, preferred_element_type=jnp.float32) for weight in whole_rows[:5])
    )
    attn_back = whole_rows[5]
    conv_back = whole_rows[6]
    query_raw, key_raw, value_raw, glu_a, glu_b = projected
    queries = row_norm(query_raw.reshape(row_count, q_local, HEAD), q_gain).astype(jnp.bfloat16)
    key_rows = (
        row_norm(key_raw.reshape(row_count, kv_local, HEAD), k_gain)
        .astype(jnp.bfloat16)
        .reshape(row_count, kv_width)
    )
    value_rows = value_raw.astype(jnp.bfloat16)
    gated_rows = (glu_a * jax.nn.sigmoid(glu_b)).astype(jnp.bfloat16)
    key_value = jnp.concatenate([key_rows, value_rows], 1)
    key_value_rim = passed_along(key_value[row_count - WINDOW :], "sp", 1)
    gated_rim = passed_along(gated_rows[row_count - (KW - 1) :], "sp", 1)
    block_count = row_count // WINDOW
    extended = jnp.concatenate([key_value_rim, key_value], 0).reshape(
        block_count + 1, WINDOW, 2 * kv_width
    )
    band = jnp.concatenate([extended[:-1], extended[1:]], 1)
    key_band = band[:, :, :kv_width].reshape(block_count, 2 * WINDOW, kv_local, HEAD)
    value_band = band[:, :, kv_width:].reshape(block_count, 2 * WINDOW, kv_local, HEAD)
    grouped = queries.reshape(block_count, WINDOW, kv_local, group_size, HEAD)
    scores = jnp.einsum(
        "nqhgd,nkhd->nhgqk", grouped, key_band, preferred_element_type=jnp.float32
    ) * HEAD ** (-0.5)
    offsets = jnp.arange(WINDOW, dtype=jnp.int32)
    band_offsets = jnp.arange(2 * WINDOW, dtype=jnp.int32)
    distance = WINDOW + offsets[:, None] - band_offsets[None, :]
    allowed = (distance >= 0) & (distance < WINDOW)
    anchor = lax.axis_index("sp") * row_count
    key_position = (
        anchor
        + jnp.arange(block_count, dtype=jnp.int32)[:, None] * WINDOW
        - WINDOW
        + band_offsets[None, :]
    )
    visible = (allowed[None, :, :] & (key_position[:, None, :] >= 0))[:, None, None]
    sink_table = sink_logit.reshape(kv_local, group_size)[None, :, :, None, None]
    masked = jnp.where(visible, scores, -jnp.inf)
    largest = jnp.maximum(jnp.max(masked, axis=-1, keepdims=True), sink_table)
    weights = jnp.where(visible, jnp.exp(scores - largest), 0.0)
    weight_sum = jnp.sum(weights, axis=-1, keepdims=True) + jnp.exp(sink_table - largest)
    log_weight = (largest + jnp.log(weight_sum))[..., 0]
    log_weight = jnp.transpose(log_weight, (1, 2, 0, 3)).reshape(q_local, row_count)
    probabilities = (weights / weight_sum).astype(jnp.bfloat16)
    attended = jnp.einsum(
        "nhgqk,nkhd->nqhgd", probabilities, value_band, preferred_element_type=jnp.float32
    )
    attended = attended.astype(jnp.bfloat16).reshape(row_count, q_local * HEAD)
    gate_extended = jnp.concatenate([gated_rim, gated_rows], 0).astype(jnp.float32)
    convolved = jnp.zeros((row_count, gated_rows.shape[1]), jnp.float32)
    for tap_index in range(KW):
        convolved = (
            convolved + conv_taps[tap_index] * gate_extended[tap_index : tap_index + row_count]
        )
    channel_sums = lax.psum(
        (jnp.sum(convolved, axis=1), jnp.sum(convolved * convolved, axis=1)), "tp"
    )
    center = (channel_sums[0] / CH)[:, None]
    spread = (channel_sums[1] / CH)[:, None] - center * center
    conv_rows = jax.nn.silu(
        (convolved - center) * lax.rsqrt(spread + EPS) * chan_gain + chan_bias
    ).astype(jnp.bfloat16)
    contract = (((1,), (1,)), ((), ()))
    result = lax.dot_general(attended, attn_back, contract, preferred_element_type=jnp.float32)
    summed = lax.psum_scatter(
        (
            result
            + lax.dot_general(conv_rows, conv_back, contract, preferred_element_type=jnp.float32)
        ).astype(jnp.bfloat16),
        "tp",
        scatter_dimension=0,
        tiled=True,
    )
    return (summed, log_weight)


def solution(mesh):
    placed = (
        P("sp", "tp"),
        P(),
        P("sp", "tp"),
        P("sp", "tp"),
        P("sp", "tp"),
        P("sp", "tp"),
        P("sp", "tp"),
        P(),
        P(),
        P("tp"),
        P(None, "tp"),
        P("tp"),
        P("tp"),
        P("sp", "tp"),
        P("sp", "tp"),
    )
    return jax.shard_map(
        local,
        mesh=mesh,
        in_specs=placed,
        out_specs=(P(("sp", "tp"), None), P("tp", "sp")),
        check_vma=False,
    )
```

profile of v0, /device:TPU:0, one launch (start us, length us, event | category | flops | bytes accessed | tf_op | source)
XLA Modules:
  0.0 476.1 jit_solution(15516827644429883974)
XLA Ops:
  7.2 0.7 all-gather.9.cloned.1.call-update
  8.0 0.7 all-gather.15.cloned.1.call-update
  8.7 0.7 all-gather.11.cloned.1.call-update
  9.5 0.5 all-gather.19.cloned.1.call-update
  10.0 0.5 all-gather.21.cloned.1.call-update
  10.6 0.5 all-gather.13.cloned.1.call-update
  11.2 0.7 all-gather.17.cloned.1.call-update
  11.9 0.7 all-gather.23.cloned.1.call-update
  12.7 0.6 fusion.80
  13.3 0.7 fusion.79
  14.3 0.3 broadcast_and_fusion
  14.7 11.3 %all-gather.9.cloned.1.call-done = bf16[1024,2048]{1,0:T(8,128)(2,1)} async-done(((bf16[1024,1024]{1,0:T(8,128)(2,1)}), bf16[1024,2048]{1,0:T(8,128)(2,1)}) %all-gather.9.cloned.1.call-update) | async-done | bytes 4194320 | tf_op jit(solution)/shard_map/all_gather | solution.py:46
  26.0 3.1 fusion
  29.1 61.3 %all-gather.15.cloned.1.call-done = bf16[2048,512]{1,0:T(8,128)(2,1)} async-done(((bf16[128,512]{1,0:T(8,128)(2,1)}), bf16[2048,512]{1,0:T(8,128)(2,1)}) %all-gather.15.cloned.1.call-update) | async-done | bytes 2097168 | tf_op jit(solution)/shard_map/all_gather | solution.py:49
  90.3 6.7 %bitcast_reduce_fusion = (f32[1024,8]{0,1:T(8,128)S(1)}, f32[1024,512]{0,1:T(8,128)}) fusion(bf16[2048,512]{1,0:T(8,128)(2,1)} %all-gather.15.cloned.1.call-done, bf16[1024,2048]{1,0:T(8,128)(2,1)} %all-gather.9.cloned.1.call-done, f32[2048]{0:T(1024)S(1)} %copy-done.28, f32[1024]{0:T(1024)S(1)} %add_rsqrt_fusion.3), kind=kOutput, calls=%fused_computation.75 | convolution fusion | flops 2156912640 | bytes 8433664 | tf_op jit(solution)/shard_map/dot_general | solution.py:58
  97.0 50.0 %all-gather.11.cloned.1.call-done = bf16[2048,256]{1,0:T(8,128)(2,1)} async-done(((bf16[128,256]{1,0:T(8,128)(2,1)}), bf16[2048,256]{1,0:T(8,128)(2,1)}) %all-gather.11.cloned.1.call-update) | async-done | bytes 1048592 | tf_op jit(solution)/shard_map/all_gather | solution.py:50
  147.0 4.0 bitcast_reduce_fusion.1
  151.1 57.8 %all-gather.19.cloned.1.call-done = bf16[2048,512]{1,0:T(8,128)(2,1)} async-done(((bf16[128,512]{1,0:T(8,128)(2,1)}), bf16[2048,512]{1,0:T(8,128)(2,1)}) %all-gather.19.cloned.1.call-update) | async-done | bytes 2097168 | tf_op jit(solution)/shard_map/all_gather | solution.py:52
  208.9 6.6 %fusion.69 = f32[1024,512]{1,0:T(8,128)} fusion(bf16[2048,512]{1,0:T(8,128)(2,1)} %all-gather.19.cloned.1.call-done, bf16[1024,2048]{1,0:T(8,128)(2,1)} %all-gather.9.cloned.1.call-done, f32[2048]{0:T(1024)S(1)} %copy-done.28, f32[1024]{0:T(1024)S(1)} %add_rsqrt_fusion.3), kind=kOutput, calls=%fused_computation.135 | convolution fusion | flops 2155872256 | bytes 8400896 | tf_op jit(solution)/shard_map/dot_general | solution.py:58
  215.5 55.2 %all-gather.21.cloned.1.call-done = bf16[2048,512]{1,0:T(8,128)(2,1)} async-done(((bf16[128,512]{1,0:T(8,128)(2,1)}), bf16[2048,512]{1,0:T(8,128)(2,1)}) %all-gather.21.cloned.1.call-update) | async-done | bytes 2097168 | tf_op jit(solution)/shard_map/all_gather | solution.py:53
  270.7 6.1 %multiply_convert_fusion.1 = bf16[1024,512]{1,0:T(8,128)(2,1)S(1)} fusion(f32[1024,512]{1,0:T(8,128)} %fusion.69, bf16[2048,512]{1,0:T(8,128)(2,1)} %all-gather.21.cloned.1.call-done, bf16[1024,2048]{1,0:T(8,128)(2,1)} %all-gather.9.cloned.1.call-done, f32[2048]{0:T(1024)S(1)} %copy-done.28, f32[1024]{0:T(1024)S(1)} %add_rsqrt_fusion.3), kind=kOutput, calls=%fused_computation.81 | convolution fusion | flops 2158493696 | bytes 9449472 | tf_op jit(solution)/shard_map/dot_general | solution.py:58
  276.8 3.4 collective-permute-start.1
  280.4 46.8 %all-gather.13.cloned.1.call-done = bf16[2048,256]{1,0:T(8,128)(2,1)} async-done(((bf16[128,256]{1,0:T(8,128)(2,1)}), bf16[2048,256]{1,0:T(8,128)(2,1)}) %all-gather.13.cloned.1.call-update) | async-done | bytes 1048592 | tf_op jit(solution)/shard_map/all_gather | solution.py:51
  327.2 4.2 convolution_convert_fusion
  331.4 0.7 fusion.58
  332.1 0.5 copy.53
  332.8 4.0 collective-permute-start
  336.8 0.3 maximum_convert_fusion
  337.3 9.5 %fusion.76 = (f32[1024]{0:T(1024)S(1)}, f32[1024]{0:T(1024)S(1)}, f32[1024,512]{1,0:T(8,128)}) fusion(f32[1054,512]{1,0:T(8,128)S(1)} %maximum_convert_fusion, f32[512]{0:T(512)S(1)} %bitcast.141, f32[512]{0:T(512)S(1)} %bitcast.142, f32[512]{0:T(512)S(1)} %bitcast.144, f32[512]{0:T(512)S(1)} %bitcast.145, f32[512]{0:T(512)S(1)} %bitcast.146, ...), kind=kLoop, calls=%fused_computation.138 | loop fusion | flops 33552384 | bytes 67180544 | tf_op jit(solution)/shard_map/reduce_sum | solution.py:116
  346.8 2.5 all-reduce
  349.3 1.3 fusion.42
  350.5 0.3 copy.52
  350.8 0.3 copy.51
  351.1 0.2 constant_dynamic-update-slice_fusion.1
  351.3 0.2 constant_dynamic-update-slice_fusion
  351.7 0.2 copy.38
  351.9 0.2 copy.37
  352.1 0.2 copy-done.25
  352.3 1.9 fusion.3
  354.3 2.2 fusion.6
  356.7 2.4 fusion.41
  359.1 0.7 copy.46
  359.8 29.5 %all-gather.17.cloned.1.call-done = bf16[2048,512]{1,0:T(8,128)(2,1)} async-done(((bf16[128,512]{1,0:T(8,128)(2,1)}), bf16[2048,512]{1,0:T(8,128)(2,1)}) %all-gather.17.cloned.1.call-update) | async-done | bytes 2097168 | tf_op jit(solution)/shard_map/all_gather | solution.py:54
  389.3 7.4 %fusion.45 = f32[1024,2048]{1,0:T(8,128)} fusion(bf16[2048,512]{1,0:T(8,128)(2,1)} %all-gather.17.cloned.1.call-done, bf16[64,8,8,128]{3,2,1,0:T(8,128)(2,1)S(1)} %bitcast.127), kind=kOutput, calls=%fused_computation.91 | convolution fusion | flops 2147483648 | bytes 11534336 | tf_op jit(solution)/shard_map/dot_general | solution.py:124
  396.7 54.6 %all-gather.23.cloned.1.call-done = bf16[2048,512]{1,0:T(8,128)(2,1)} async-done(((bf16[128,512]{1,0:T(8,128)(2,1)}), bf16[2048,512]{1,0:T(8,128)(2,1)}) %all-gather.23.cloned.1.call-update) | async-done | bytes 2097168 | tf_op jit(solution)/shard_map/all_gather | solution.py:55
  451.2 7.3 %add_convert_fusion = bf16[1024,2048]{1,0:T(8,128)(2,1)} fusion(f32[1024,2048]{1,0:T(8,128)} %fusion.45, bf16[2048,512]{1,0:T(8,128)(2,1)} %all-gather.23.cloned.1.call-done, f32[1024,512]{1,0:T(8,128)S(1)} %copy-done, f32[512]{0:T(512)S(1)} %copy-done.29, f32[512]{0:T(512)S(1)} %copy-done.30, f32[1024]{0:T(1024)S(1)} %get-tuple-element.43, ...), kind=kOutput, calls=%fused_computation.10 | convolution fusion | flops 2156396544 | bytes 16789504 | tf_op jit(solution)/shard_map/dot_general | solution.py:128
  458.7 0.6 copy.76
  459.3 10.3 %reduce-scatter.2.cloned.1.call-done = bf16[512,2048]{1,0:T(8,128)(2,1)} async-done(((bf16[1024,2048]{1,0:T(8,128)(2,1)}), bf16[512,2048]{1,0:T(8,128)(2,1)}) %reduce-scatter.2.cloned.1.call-update) | async-done | bytes 2097168 | tf_op jit(solution)/shard_map/reduce_scatter | solution.py:125
  (92 shorter events, 1.5 us)
Async XLA Ops:
  7.2 5.6 %copy-start.4 = (f32[31,512]{1,0:T(8,128)S(1)}, f32[31,512]{1,0:T(8,128)}, u32[]{:S(2)}) copy-start(f32[31,512]{1,0:T(8,128)} %param.25) | copy-start | bytes 190468
  7.2 6.9 %copy-start.26 = (f32[8]{0:T(128)S(1)}, f32[8]{0:T(128)}, u32[]{:S(2)}) copy-start(f32[8]{0:T(128)} %param.24) | copy-start | bytes 100
  7.2 7.0 %copy-start.27 = (f32[64]{0:T(128)S(1)}, f32[64]{0:T(128)}, u32[]{:S(2)}) copy-start(f32[64]{0:T(128)} %param.23) | copy-start | bytes 772
  7.2 18.8 %all-gather.9.cloned.1.call-start = ((), (), s32[]{:S(2)}) async-start(), calls=%async_computation.1 | async-start | bytes 6291456 | tf_op jit(solution)/shard_map/all_gather | solution.py:46
  7.9 82.4 %all-gather.15.cloned.1.call-start = ((), (), s32[]{:S(2)}) async-start(), calls=%async_computation.4 | async-start | bytes 2228224 | tf_op jit(solution)/shard_map/all_gather | solution.py:49
  8.7 138.3 %all-gather.11.cloned.1.call-start = ((), (), s32[]{:S(2)}) async-start(), calls=%async_computation.2 | async-start | bytes 1114112 | tf_op jit(solution)/shard_map/all_gather | solution.py:50
  9.4 199.5 %all-gather.19.cloned.1.call-start = ((), (), s32[]{:S(2)}) async-start(), calls=%async_computation.6 | async-start | bytes 2228224 | tf_op jit(solution)/shard_map/all_gather | solution.py:52
  10.0 260.7 %all-gather.21.cloned.1.call-start = ((), (), s32[]{:S(2)}) async-start(), calls=%async_computation.7 | async-start | bytes 2228224 | tf_op jit(solution)/shard_map/all_gather | solution.py:53
  10.6 316.7 %all-gather.13.cloned.1.call-start = ((), (), s32[]{:S(2)}) async-start(), calls=%async_computation.3 | async-start | bytes 1114112 | tf_op jit(solution)/shard_map/all_gather | solution.py:51
  11.2 378.1 %all-gather.17.cloned.1.call-start = ((), (), s32[]{:S(2)}) async-start(), calls=%async_computation.5 | async-start | bytes 2228224 | tf_op jit(solution)/shard_map/all_gather | solution.py:54
  11.9 439.3 %all-gather.23.cloned.1.call-start = ((), (), s32[]{:S(2)}) async-start(), calls=%async_computation.8 | async-start | bytes 2228224 | tf_op jit(solution)/shard_map/all_gather | solution.py:55
  12.7 457.0 %reduce-scatter.2.cloned.1.call-start = ((), (), s32[]{:S(2)}) async-start(), calls=%async_computation.9 | async-start | bytes 6291456 | tf_op jit(solution)/shard_map/reduce_scatter | solution.py:125
  14.6 75.7 %copy-start.28 = (f32[2048]{0:T(1024)S(1)}, f32[2048]{0:T(1024)}, u32[]{:S(2)}) copy-start(f32[2048]{0:T(1024)} %param.16) | copy-start | bytes 24580
  276.8 3.4 copy-start.2
  276.8 59.9 %collective-permute-start.1 = (bf16[30,512]{1,0:T(8,128)(2,1)S(1)}, bf16[30,512]{1,0:T(8,128)(2,1)S(1)}, u32[]{:S(2)}, u32[]{:S(2)}) collective-permute-start(bf16[30,512]{1,0:T(8,128)(2,1)S(1)} %slice.281), channel_id=1, source_target_pairs={{0,2},{2,4},{4,6},{6,8},{8,10},{10,12},{12,14},{14,16},{16,18},{18... | collective-permute-start | bytes 92168 | tf_op jit(solution)/shard_map/ppermute | solution.py:16
  327.2 4.9 %copy-start.1 = (f32[1024,512]{0,1:T(8,128)S(1)}, f32[1024,512]{0,1:T(8,128)}, u32[]{:S(2)}) copy-start(f32[1024,512]{0,1:T(8,128)} %get-tuple-element.47) | copy-start | bytes 6291460
  332.1 4.7 copy-start.3
  332.6 4.6 copy-start.5
  332.6 4.6 copy-start.6
  332.6 4.6 copy-start.7
  332.6 4.6 copy-start.8
  332.6 4.6 copy-start.9
  332.6 4.6 copy-start.10
  332.6 4.6 copy-start.11
  332.6 4.6 copy-start.12
  332.7 4.6 copy-start.13
  332.7 4.6 copy-start.14
  332.7 4.6 copy-start.15
  332.7 4.6 copy-start.16
  332.7 4.6 copy-start.17
  332.7 4.6 copy-start.18
  332.7 4.6 copy-start.19
  332.7 4.6 copy-start.20
  332.7 4.6 copy-start.21
  332.7 4.6 copy-start.22
  332.8 4.6 copy-start.23
  332.8 4.6 copy-start.24
  332.8 16.5 %collective-permute-start = (bf16[128,512]{0,1:T(8,128)(2,1)}, bf16[128,512]{0,1:T(8,128)(2,1)}, u32[]{:S(2)}, u32[]{:S(2)}) collective-permute-start(bf16[128,512]{0,1:T(8,128)(2,1)} %fusion.58), channel_id=1, source_target_pairs={{0,2},{2,4},{4,6},{6,8},{8,10},{10,12},{12,14},{14,16},{16,18},{18... | collective-permute-start | bytes 393224 | tf_op jit(solution)/shard_map/ppermute | solution.py:16
  351.7 0.7 copy-start.25
  389.3 62.0 %copy-start = (f32[1024,512]{1,0:T(8,128)S(1)}, f32[1024,512]{1,0:T(8,128)}, u32[]{:S(2)}) copy-start(f32[1024,512]{1,0:T(8,128)} %get-tuple-element.6) | copy-start | bytes 6291460
  389.3 62.0 %copy-start.29 = (f32[512]{0:T(512)S(1)}, f32[512]{0:T(512)}, u32[]{:S(2)}) copy-start(f32[512]{0:T(512)} %param.27) | copy-start | bytes 6148
  389.3 62.0 %copy-start.30 = (f32[512]{0:T(512)S(1)}, f32[512]{0:T(512)}, u32[]{:S(2)}) copy-start(f32[512]{0:T(512)} %param.26) | copy-start | bytes 6148
Sparse Core Ops, SparseCore 0:
  9.5 16.3 all-gather.8
  28.7 61.5 all-gather.14
  93.1 53.8 all-gather.10
  149.6 59.2 all-gather.18
  211.5 59.1 all-gather.20
  273.3 53.8 all-gather.12
  330.0 59.2 all-gather.16
  392.0 59.1 all-gather.22
  458.7 10.8 reduce-scatter.1
where the time goes:
time: 476 us
  waiting for transfers between devices  382 us (80%)
  matrix products  46.7 us (10%)
  other arithmetic  18 us (4%)
  between operations  14.4 us (3%)
  starting transfers between devices  7.71 us (2%)
  local copies, waits for them, and re-layouts  5.14 us (1%)
    all_gather x1, waiting for transfers between devices, local(): lax.all_gather(w_query, 'sp', axis=0, tiled=True)  61.3 us
    all_gather x1, waiting for transfers between devices, local(): lax.all_gather(w_glu_a, 'sp', axis=0, tiled=True)  57.8 us
    all_gather x1, waiting for transfers between devices, local(): lax.all_gather(w_glu_b, 'sp', axis=0, tiled=True)  55.2 us
    all_gather x1, waiting for transfers between devices, local(): lax.all_gather(w_conv_back, 'sp', axis=0, tiled=True)  54.6 us
    all_gather x1, waiting for transfers between devices, local(): lax.all_gather(w_key, 'sp', axis=0, tiled=True)  50 us
    all_gather x1, waiting for transfers between devices, local(): lax.all_gather(w_value, 'sp', axis=0, tiled=True)  46.8 us
    all_gather x1, waiting for transfers between devices, local(): lax.all_gather(w_attn_back, 'sp', axis=0, tiled=True)  29.5 us
    dot_general x5, matrix products, local(): jnp.dot(normed, weight, preferred_element_type=jnp.float32)  27.6 us
  transfers between devices with their start and end apart: 11, of which 9 were waited for; matrix products, arithmetic and copies ran while one was open for 13% of the time, Pallas kernels for 0%

commit v1 on v0

--- a/solution.py
+++ b/solution.py
@@ -45,10 +45,19 @@
     kv_width = kv_local * HEAD
     gathered = lax.all_gather(tokens, "tp", axis=1, tiled=True)
     normed = row_norm(gathered.astype(jnp.float32), norm_gain).astype(jnp.bfloat16)
+    serve_set = lambda s0: jnp.concatenate(
+        lax.all_to_all(
+            jnp.stack(lax.psum(1, axis_name="sp") * [s0], axis=0),
+            split_axis=0,
+            concat_axis=0,
+            axis_name="sp",
+        ),
+        axis=0,
+    )
     whole_rows = (
         lax.all_gather(w_query, "sp", axis=0, tiled=True),
         lax.all_gather(w_key, "sp", axis=0, tiled=True),
-        lax.all_gather(w_value, "sp", axis=0, tiled=True),
+        serve_set(w_value),
         lax.all_gather(w_glu_a, "sp", axis=0, tiled=True),
         lax.all_gather(w_glu_b, "sp", axis=0, tiled=True),
         lax.all_gather(w_attn_back, "sp", axis=0, tiled=True),

time: 476 us -> 420 us (0.88)
  waiting for transfers between devices: 382 us -> 316 us
  starting transfers between devices: 7.71 us -> 15.8 us
    all_gather x1 -> x0, waiting for transfers between devices: 46.8 us -> none  [local(): lax.all_gather(w_value, 'sp', axis=0, tiled=True)]
    all_gather x1, waiting for transfers between devices: 11.3 us -> 2.58 us  [local(): gathered = lax.all_gather(tokens, 'tp', axis=1, tiled=True)]
    all_to_all x0 -> x1, starting transfers between devices: none -> 8.34 us  [local(): lax.all_to_all(jnp.stack(lax.psum(1, axis_name='sp') * [s0], axis=0), spl...]
    all_gather x1, waiting for transfers between devices: 29.5 us -> 23.1 us  [local(): lax.all_gather(w_attn_back, 'sp', axis=0, tiled=True)]
  transfers between devices with their start and end apart: 11 -> 11, of which waited for: 9 -> 8; matrix products, arithmetic and copies ran while one was open for 13% -> 15% of each run, Pallas kernels for 0% -> 0%
where the time goes in v1:
time: 420 us
  waiting for transfers between devices  316 us (75%)
  matrix products  46.3 us (11%)
  other arithmetic  18 us (4%)
  starting transfers between devices  15.8 us (4%)
  between operations  14.8 us (4%)
  local copies, waits for them, and re-layouts  7.23 us (2%)
    all_gather x1, waiting for transfers between devices, local(): lax.all_gather(w_glu_a, 'sp', axis=0, tiled=True)  61.5 us
    all_gather x1, waiting for transfers between devices, local(): lax.all_gather(w_query, 'sp', axis=0, tiled=True)  57.6 us
    all_gather x1, waiting for transfers between devices, local(): lax.all_gather(w_glu_b, 'sp', axis=0, tiled=True)  55.4 us
    all_gather x1, waiting for transfers between devices, local(): lax.all_gather(w_conv_back, 'sp', axis=0, tiled=True)  54.6 us
    all_gather x1, waiting for transfers between devices, local(): lax.all_gather(w_key, 'sp', axis=0, tiled=True)  46 us
    dot_general x5, matrix products, local(): jnp.dot(normed, weight, preferred_element_type=jnp.float32)  27.2 us
    all_gather x1, waiting for transfers between devices, local(): lax.all_gather(w_attn_back, 'sp', axis=0, tiled=True)  23.1 us
    reduce_scatter x1, waiting for transfers between devices, local(): lax.psum_scatter((result + lax.dot_general(conv_rows, conv_back, contract...  10.3 us
  transfers between devices with their start and end apart: 11, of which 8 were waited for; matrix products, arithmetic and copies ran while one was open for 15% of the time, Pallas kernels for 0%

profile of v1, /device:TPU:0, one launch (start us, length us, event | category | flops | bytes accessed | tf_op | source)
XLA Modules:
  0.0 420.1 jit_solution(7888146449241350972)
XLA Ops:
  7.2 0.7 all-gather.8.cloned.1.call-update
  8.0 0.7 all-gather.16.cloned.1.call-update
  8.7 0.7 all-gather.18.cloned.1.call-update
  9.5 0.5 all-gather.10.cloned.1.call-update
  10.0 0.5 all-gather.12.cloned.1.call-update
  10.6 0.5 all-gather.14.cloned.1.call-update
  11.2 1.1 stack.2
  12.2 8.3 %all-to-all-start = ((bf16[16,128,256]{2,1,0:T(8,128)(2,1)}), bf16[16,128,256]{2,1,0:T(8,128)(2,1)S(1)}, u32[]{:S(2)}, u32[]{:S(2)}) async-start(bf16[16,128,256]{2,1,0:T(8,128)(2,1)} %stack.2), calls=%async_computation | async-start | bytes 2097152 | tf_op jit(solution)/shard_map/all_to_all | solution.py:49
  20.6 0.7 all-gather.20.cloned.1.call-update
  21.4 0.6 fusion.80
  22.0 0.7 fusion.79
  23.0 0.3 broadcast_and_fusion
  23.4 2.6 all-gather.8.cloned.1.call-done
  25.9 3.1 fusion
  29.0 61.5 %all-gather.16.cloned.1.call-done = bf16[2048,512]{1,0:T(8,128)(2,1)} async-done(((bf16[128,512]{1,0:T(8,128)(2,1)}), bf16[2048,512]{1,0:T(8,128)(2,1)}) %all-gather.16.cloned.1.call-update) | async-done | bytes 2097168 | tf_op jit(solution)/shard_map/all_gather | solution.py:61
  90.6 6.6 %fusion.69 = f32[1024,512]{1,0:T(8,128)} fusion(bf16[2048,512]{1,0:T(8,128)(2,1)} %all-gather.16.cloned.1.call-done, bf16[1024,2048]{1,0:T(8,128)(2,1)} %all-gather.8.cloned.1.call-done, f32[2048]{0:T(1024)S(1)} %copy-done.30, f32[1024]{0:T(1024)S(1)} %add_rsqrt_fusion.3), kind=kOutput, calls=%fused_computation.135 | convolution fusion | flops 2155872256 | bytes 8400896 | tf_op jit(solution)/shard_map/dot_general | solution.py:67
  97.2 55.4 %all-gather.18.cloned.1.call-done = bf16[2048,512]{1,0:T(8,128)(2,1)} async-done(((bf16[128,512]{1,0:T(8,128)(2,1)}), bf16[2048,512]{1,0:T(8,128)(2,1)}) %all-gather.18.cloned.1.call-update) | async-done | bytes 2097168 | tf_op jit(solution)/shard_map/all_gather | solution.py:62
  152.6 6.1 %multiply_convert_fusion.1 = bf16[1024,512]{1,0:T(8,128)(2,1)S(1)} fusion(f32[1024,512]{1,0:T(8,128)} %fusion.69, bf16[2048,512]{1,0:T(8,128)(2,1)} %all-gather.18.cloned.1.call-done, bf16[1024,2048]{1,0:T(8,128)(2,1)} %all-gather.8.cloned.1.call-done, f32[2048]{0:T(1024)S(1)} %copy-done.30, f32[1024]{0:T(1024)S(1)} %add_rsqrt_fusion.3), kind=kOutput, calls=%fused_computation.81 | convolution fusion | flops 2158493696 | bytes 9449472 | tf_op jit(solution)/shard_map/dot_general | solution.py:67
  158.7 1.0 copy-done.2
  159.7 3.4 collective-permute-start.1
  163.1 46.0 %all-gather.10.cloned.1.call-done = bf16[2048,256]{1,0:T(8,128)(2,1)} async-done(((bf16[128,256]{1,0:T(8,128)(2,1)}), bf16[2048,256]{1,0:T(8,128)(2,1)}) %all-gather.10.cloned.1.call-update) | async-done | bytes 1048592 | tf_op jit(solution)/shard_map/all_gather | solution.py:59
  209.1 4.0 bitcast_reduce_fusion.1
  213.4 57.6 %all-gather.12.cloned.1.call-done = bf16[2048,512]{1,0:T(8,128)(2,1)} async-done(((bf16[128,512]{1,0:T(8,128)(2,1)}), bf16[2048,512]{1,0:T(8,128)(2,1)}) %all-gather.12.cloned.1.call-update) | async-done | bytes 2097168 | tf_op jit(solution)/shard_map/all_gather | solution.py:58
  271.0 6.7 %bitcast_reduce_fusion = (f32[1024,8]{0,1:T(8,128)S(1)}, f32[1024,512]{0,1:T(8,128)}) fusion(bf16[2048,512]{1,0:T(8,128)(2,1)} %all-gather.12.cloned.1.call-done, bf16[1024,2048]{1,0:T(8,128)(2,1)} %all-gather.8.cloned.1.call-done, f32[2048]{0:T(1024)S(1)} %copy-done.30, f32[1024]{0:T(1024)S(1)} %add_rsqrt_fusion.3), kind=kOutput, calls=%fused_computation.75 | convolution fusion | flops 2156912640 | bytes 8433664 | tf_op jit(solution)/shard_map/dot_general | solution.py:67
  277.7 3.9 convolution_convert_fusion
  281.6 0.7 fusion.58
  282.3 0.5 copy.53
  282.9 3.8 collective-permute-start
  286.8 0.3 maximum_convert_fusion
  287.3 9.5 %fusion.76 = (f32[1024]{0:T(1024)S(1)}, f32[1024]{0:T(1024)S(1)}, f32[1024,512]{1,0:T(8,128)}) fusion(f32[1054,512]{1,0:T(8,128)S(1)} %maximum_convert_fusion, f32[512]{0:T(512)S(1)} %bitcast.143, f32[512]{0:T(512)S(1)} %bitcast.144, f32[512]{0:T(512)S(1)} %bitcast.146, f32[512]{0:T(512)S(1)} %bitcast.147, f32[512]{0:T(512)S(1)} %bitcast.148, ...), kind=kLoop, calls=%fused_computation.138 | loop fusion | flops 33552384 | bytes 67180544 | tf_op jit(solution)/shard_map/reduce_sum | solution.py:125
  296.8 2.5 all-reduce
  299.2 1.3 fusion.42
  300.5 0.3 copy.52
  300.8 0.3 copy.51
  301.3 0.2 constant_dynamic-update-slice_fusion
  301.7 0.2 copy.38
  301.9 0.2 copy.37
  302.1 0.2 copy-done.27
  302.3 1.9 fusion.3
  304.3 2.2 fusion.6
  306.7 2.4 fusion.41
  309.1 0.7 copy.46
  309.8 23.1 %all-gather.14.cloned.1.call-done = bf16[2048,512]{1,0:T(8,128)(2,1)} async-done(((bf16[128,512]{1,0:T(8,128)(2,1)}), bf16[2048,512]{1,0:T(8,128)(2,1)}) %all-gather.14.cloned.1.call-update) | async-done | bytes 2097168 | tf_op jit(solution)/shard_map/all_gather | solution.py:63
  332.9 7.4 %fusion.45 = f32[1024,2048]{1,0:T(8,128)} fusion(bf16[2048,512]{1,0:T(8,128)(2,1)} %all-gather.14.cloned.1.call-done, bf16[64,8,8,128]{3,2,1,0:T(8,128)(2,1)S(1)} %bitcast.129), kind=kOutput, calls=%fused_computation.91 | convolution fusion | flops 2147483648 | bytes 11534336 | tf_op jit(solution)/shard_map/dot_general | solution.py:133
  340.3 54.6 %all-gather.20.cloned.1.call-done = bf16[2048,512]{1,0:T(8,128)(2,1)} async-done(((bf16[128,512]{1,0:T(8,128)(2,1)}), bf16[2048,512]{1,0:T(8,128)(2,1)}) %all-gather.20.cloned.1.call-update) | async-done | bytes 2097168 | tf_op jit(solution)/shard_map/all_gather | solution.py:64
  394.9 7.3 %add_convert_fusion = bf16[1024,2048]{1,0:T(8,128)(2,1)} fusion(f32[1024,2048]{1,0:T(8,128)} %fusion.45, bf16[2048,512]{1,0:T(8,128)(2,1)} %all-gather.20.cloned.1.call-done, f32[1024,512]{1,0:T(8,128)S(1)} %copy-done, f32[512]{0:T(512)S(1)} %copy-done.32, f32[512]{0:T(512)S(1)} %copy-done.33, f32[1024]{0:T(1024)S(1)} %get-tuple-element.43, ...), kind=kOutput, calls=%fused_computation.10 | convolution fusion | flops 2156396544 | bytes 16789504 | tf_op jit(solution)/shard_map/dot_general | solution.py:137
  402.4 0.6 copy.76
  403.0 10.3 %reduce-scatter.2.cloned.1.call-done = bf16[512,2048]{1,0:T(8,128)(2,1)} async-done(((bf16[1024,2048]{1,0:T(8,128)(2,1)}), bf16[512,2048]{1,0:T(8,128)(2,1)}) %reduce-scatter.2.cloned.1.call-update) | async-done | bytes 2097168 | tf_op jit(solution)/shard_map/reduce_scatter | solution.py:134
  (98 shorter events, 1.6 us)
Async XLA Ops:
  7.2 4.0 copy-start.4
  7.2 18.8 %all-gather.8.cloned.1.call-start = ((), (), s32[]{:S(2)}) async-start(), calls=%async_computation.2 | async-start | bytes 6291456 | tf_op jit(solution)/shard_map/all_gather | solution.py:46
  7.9 13.5 %copy-start.5 = (f32[31,512]{1,0:T(8,128)S(1)}, f32[31,512]{1,0:T(8,128)}, u32[]{:S(2)}) copy-start(f32[31,512]{1,0:T(8,128)} %param.25) | copy-start | bytes 190468
  7.9 14.9 %copy-start.28 = (f32[8]{0:T(128)S(1)}, f32[8]{0:T(128)}, u32[]{:S(2)}) copy-start(f32[8]{0:T(128)} %param.24) | copy-start | bytes 100
  7.9 15.0 %copy-start.29 = (f32[64]{0:T(128)S(1)}, f32[64]{0:T(128)}, u32[]{:S(2)}) copy-start(f32[64]{0:T(128)} %param.23) | copy-start | bytes 772
  7.9 82.7 %all-gather.16.cloned.1.call-start = ((), (), s32[]{:S(2)}) async-start(), calls=%async_computation.6 | async-start | bytes 2228224 | tf_op jit(solution)/shard_map/all_gather | solution.py:61
  8.7 143.9 %all-gather.18.cloned.1.call-start = ((), (), s32[]{:S(2)}) async-start(), calls=%async_computation.7 | async-start | bytes 2228224 | tf_op jit(solution)/shard_map/all_gather | solution.py:62
  9.4 199.7 %all-gather.10.cloned.1.call-start = ((), (), s32[]{:S(2)}) async-start(), calls=%async_computation.3 | async-start | bytes 1114112 | tf_op jit(solution)/shard_map/all_gather | solution.py:59
  10.0 261.0 %all-gather.12.cloned.1.call-start = ((), (), s32[]{:S(2)}) async-start(), calls=%async_computation.4 | async-start | bytes 2228224 | tf_op jit(solution)/shard_map/all_gather | solution.py:58
  10.6 322.3 %all-gather.14.cloned.1.call-start = ((), (), s32[]{:S(2)}) async-start(), calls=%async_computation.5 | async-start | bytes 2228224 | tf_op jit(solution)/shard_map/all_gather | solution.py:63
  12.2 265.4 %all-to-all-start = ((bf16[16,128,256]{2,1,0:T(8,128)(2,1)}), bf16[16,128,256]{2,1,0:T(8,128)(2,1)S(1)}, u32[]{:S(2)}, u32[]{:S(2)}) async-start(bf16[16,128,256]{2,1,0:T(8,128)(2,1)} %stack.2), calls=%async_computation | async-start | bytes 2097152 | tf_op jit(solution)/shard_map/all_to_all | solution.py:49
  20.6 374.3 %all-gather.20.cloned.1.call-start = ((), (), s32[]{:S(2)}) async-start(), calls=%async_computation.8 | async-start | bytes 2228224 | tf_op jit(solution)/shard_map/all_gather | solution.py:64
  21.4 391.9 %reduce-scatter.2.cloned.1.call-start = ((), (), s32[]{:S(2)}) async-start(), calls=%async_computation.9 | async-start | bytes 6291456 | tf_op jit(solution)/shard_map/reduce_scatter | solution.py:134
  23.4 67.2 %copy-start.30 = (f32[2048]{0:T(1024)S(1)}, f32[2048]{0:T(1024)}, u32[]{:S(2)}) copy-start(f32[2048]{0:T(1024)} %param.16) | copy-start | bytes 24580
  29.0 241.9 %copy-start.26 = (f32[1024]{0:T(1024)}, f32[1024]{0:T(1024)S(1)}, u32[]{:S(2)}) copy-start(f32[1024]{0:T(1024)S(1)} %add_rsqrt_fusion.3) | copy-start | bytes 12292
  158.7 1.0 copy-start.2
  159.7 127.1 %collective-permute-start.1 = (bf16[30,512]{1,0:T(8,128)(2,1)S(1)}, bf16[30,512]{1,0:T(8,128)(2,1)S(1)}, u32[]{:S(2)}, u32[]{:S(2)}) collective-permute-start(bf16[30,512]{1,0:T(8,128)(2,1)S(1)} %slice.281), channel_id=1, source_target_pairs={{0,2},{2,4},{4,6},{6,8},{8,10},{10,12},{12,14},{14,16},{16,18},{18... | collective-permute-start | bytes 92168 | tf_op jit(solution)/shard_map/ppermute | solution.py:16
  213.3 64.4 %copy-start.31 = (f32[2048]{0:T(1024)S(1)}, f32[2048]{0:T(1024)}, u32[]{:S(2)}) copy-start(f32[2048]{0:T(1024)} %param.16) | copy-start | bytes 24580
  277.7 4.5 %copy-start.1 = (f32[1024,512]{0,1:T(8,128)S(1)}, f32[1024,512]{0,1:T(8,128)}, u32[]{:S(2)}) copy-start(f32[1024,512]{0,1:T(8,128)} %get-tuple-element.47) | copy-start | bytes 6291460
  282.3 4.5 %copy-start.3 = (bf16[1024,512]{1,0:T(8,128)(2,1)S(1)}, bf16[1024,512]{1,0:T(8,128)(2,1)}, u32[]{:S(2)}) copy-start(bf16[1024,512]{1,0:T(8,128)(2,1)} %copy-done.2) | copy-start | bytes 3145732
  282.7 4.4 %copy-start.6 = (f32[1,512]{1,0:T(1,128)S(1)}, f32[1,512]{1,0:T(1,128)}, u32[]{:S(2)}) copy-start(f32[1,512]{1,0:T(1,128)} %get-tuple-element.41) | copy-start | bytes 6148
  282.7 4.4 %copy-start.7 = (f32[1,512]{1,0:T(1,128)S(1)}, f32[1,512]{1,0:T(1,128)}, u32[]{:S(2)}) copy-start(f32[1,512]{1,0:T(1,128)} %get-tuple-element.11) | copy-start | bytes 6148
  282.8 4.4 %copy-start.8 = (f32[1,512]{1,0:T(1,128)S(1)}, f32[1,512]{1,0:T(1,128)}, u32[]{:S(2)}) copy-start(f32[1,512]{1,0:T(1,128)} %get-tuple-element.12) | copy-start | bytes 6148
  282.8 4.4 %copy-start.9 = (f32[1,512]{1,0:T(1,128)S(1)}, f32[1,512]{1,0:T(1,128)}, u32[]{:S(2)}) copy-start(f32[1,512]{1,0:T(1,128)} %get-tuple-element.13) | copy-start | bytes 6148
  282.8 4.4 %copy-start.10 = (f32[1,512]{1,0:T(1,128)S(1)}, f32[1,512]{1,0:T(1,128)}, u32[]{:S(2)}) copy-start(f32[1,512]{1,0:T(1,128)} %get-tuple-element.14) | copy-start | bytes 6148
  282.8 4.4 %copy-start.11 = (f32[1,512]{1,0:T(1,128)S(1)}, f32[1,512]{1,0:T(1,128)}, u32[]{:S(2)}) copy-start(f32[1,512]{1,0:T(1,128)} %get-tuple-element.15) | copy-start | bytes 6148
  282.8 4.4 %copy-start.12 = (f32[1,512]{1,0:T(1,128)S(1)}, f32[1,512]{1,0:T(1,128)}, u32[]{:S(2)}) copy-start(f32[1,512]{1,0:T(1,128)} %get-tuple-element.16) | copy-start | bytes 6148
  282.8 4.4 %copy-start.13 = (f32[1,512]{1,0:T(1,128)S(1)}, f32[1,512]{1,0:T(1,128)}, u32[]{:S(2)}) copy-start(f32[1,512]{1,0:T(1,128)} %get-tuple-element.17) | copy-start | bytes 6148
  282.8 4.4 %copy-start.14 = (f32[1,512]{1,0:T(1,128)S(1)}, f32[1,512]{1,0:T(1,128)}, u32[]{:S(2)}) copy-start(f32[1,512]{1,0:T(1,128)} %get-tuple-element.18) | copy-start | bytes 6148
  282.8 4.4 %copy-start.15 = (f32[1,512]{1,0:T(1,128)S(1)}, f32[1,512]{1,0:T(1,128)}, u32[]{:S(2)}) copy-start(f32[1,512]{1,0:T(1,128)} %get-tuple-element.19) | copy-start | bytes 6148
  282.8 4.4 %copy-start.16 = (f32[1,512]{1,0:T(1,128)S(1)}, f32[1,512]{1,0:T(1,128)}, u32[]{:S(2)}) copy-start(f32[1,512]{1,0:T(1,128)} %get-tuple-element.20) | copy-start | bytes 6148
  282.8 4.4 %copy-start.17 = (f32[1,512]{1,0:T(1,128)S(1)}, f32[1,512]{1,0:T(1,128)}, u32[]{:S(2)}) copy-start(f32[1,512]{1,0:T(1,128)} %get-tuple-element.21) | copy-start | bytes 6148
  282.9 4.4 %copy-start.18 = (f32[1,512]{1,0:T(1,128)S(1)}, f32[1,512]{1,0:T(1,128)}, u32[]{:S(2)}) copy-start(f32[1,512]{1,0:T(1,128)} %get-tuple-element.22) | copy-start | bytes 6148
  282.9 4.4 %copy-start.19 = (f32[1,512]{1,0:T(1,128)S(1)}, f32[1,512]{1,0:T(1,128)}, u32[]{:S(2)}) copy-start(f32[1,512]{1,0:T(1,128)} %get-tuple-element.23) | copy-start | bytes 6148
  282.9 4.4 %copy-start.20 = (f32[1,512]{1,0:T(1,128)S(1)}, f32[1,512]{1,0:T(1,128)}, u32[]{:S(2)}) copy-start(f32[1,512]{1,0:T(1,128)} %get-tuple-element.24) | copy-start | bytes 6148
  282.9 4.4 %copy-start.21 = (f32[1,512]{1,0:T(1,128)S(1)}, f32[1,512]{1,0:T(1,128)}, u32[]{:S(2)}) copy-start(f32[1,512]{1,0:T(1,128)} %get-tuple-element.25) | copy-start | bytes 6148
  282.9 4.4 %copy-start.22 = (f32[1,512]{1,0:T(1,128)S(1)}, f32[1,512]{1,0:T(1,128)}, u32[]{:S(2)}) copy-start(f32[1,512]{1,0:T(1,128)} %get-tuple-element.26) | copy-start | bytes 6148
  282.9 4.4 %copy-start.23 = (f32[1,512]{1,0:T(1,128)S(1)}, f32[1,512]{1,0:T(1,128)}, u32[]{:S(2)}) copy-start(f32[1,512]{1,0:T(1,128)} %get-tuple-element.27) | copy-start | bytes 6148
  282.9 4.4 %copy-start.24 = (f32[1,512]{1,0:T(1,128)S(1)}, f32[1,512]{1,0:T(1,128)}, u32[]{:S(2)}) copy-start(f32[1,512]{1,0:T(1,128)} %get-tuple-element.28) | copy-start | bytes 6148
  282.9 4.4 %copy-start.25 = (f32[1,512]{1,0:T(1,128)S(1)}, f32[1,512]{1,0:T(1,128)}, u32[]{:S(2)}) copy-start(f32[1,512]{1,0:T(1,128)} %get-tuple-element.29) | copy-start | bytes 6148
  282.9 16.3 %collective-permute-start = (bf16[128,512]{0,1:T(8,128)(2,1)}, bf16[128,512]{0,1:T(8,128)(2,1)}, u32[]{:S(2)}, u32[]{:S(2)}) collective-permute-start(bf16[128,512]{0,1:T(8,128)(2,1)} %fusion.58), channel_id=1, source_target_pairs={{0,2},{2,4},{4,6},{6,8},{8,10},{10,12},{12,14},{14,16},{16,18},{18... | collective-permute-start | bytes 393224 | tf_op jit(solution)/shard_map/ppermute | solution.py:16
  301.7 0.7 copy-start.27
  332.9 62.0 %copy-start = (f32[1024,512]{1,0:T(8,128)S(1)}, f32[1024,512]{1,0:T(8,128)}, u32[]{:S(2)}) copy-start(f32[1024,512]{1,0:T(8,128)} %get-tuple-element.6) | copy-start | bytes 6291460
  332.9 62.0 %copy-start.32 = (f32[512]{0:T(512)S(1)}, f32[512]{0:T(512)}, u32[]{:S(2)}) copy-start(f32[512]{0:T(512)} %param.27) | copy-start | bytes 6148
  332.9 62.0 %copy-start.33 = (f32[512]{0:T(512)S(1)}, f32[512]{0:T(512)}, u32[]{:S(2)}) copy-start(f32[512]{0:T(512)} %param.26) | copy-start | bytes 6148
Sparse Core Ops, SparseCore 0:
  9.5 16.3 all-gather.7
  28.7 61.8 all-gather.15
  93.4 59.1 all-gather.17
  155.2 53.8 all-gather.9
  211.7 59.2 all-gather.11
  273.6 59.2 all-gather.13
  335.7 59.1 all-gather.19
  402.4 10.8 reduce-scatter.1
